TPU v7x, 32 devices: a whole 2x2x4 slice. The times are simulated.
32 devices in a mesh: ra: 4 (over z), cb: 8 (over y, x, core).
Axes of the slice: x: 2, y: 2, z: 4, core: 2. Of those that a mesh axis runs over, the one named last changes fastest.
Arguments:
- tokens: bfloat16 [2, 128, 3072], P(None, None, 'ra'), may hold values from -70 to 70
- norm_gain: float32 [2, 3072], P(None, 'ra'), may hold values from 0.1 to 1.9
- gate_weight: float32 [2, 3072, 8448], P(None, 'ra', 'cb'), may hold values from -0.109375 to 0.109375
- gate_scale: float32 [2, 8448], P(None, 'cb'), may hold values from 0.5 to 2
- up_weight: float32 [2, 3072, 8448], P(None, 'ra', 'cb'), may hold values from -0.109375 to 0.109375
- up_scale: float32 [2, 8448], P(None, 'cb'), may hold values from 0.5 to 2
- conv_weight: float32 [2, 3, 8448], P(None, None, 'cb'), may hold values from -3.5 to 3.5
- conv_bias: float32 [2, 8448], P(None, 'cb'), may hold values from -3 to 3
- down_weight: float32 [2, 8448, 3072], P(None, 'cb', 'ra'), may hold values from -0.0625 to 0.0625
- down_scale: float32 [2, 3072], P(None, 'ra'), may hold values from 0.5 to 2
Outputs:
- layer_output: bfloat16 [2, 128, 3072], P(None, None, 'ra')
All inputs are finite; a program needn't handle non-finite values.
Results may differ from a plain program's by a relative error of at most 0.014.
Values may be sent and summed in bfloat16 or wider, within the bound.
A program may use at most 64 MiB of HBM per device.

v0:
```python
import jax
import jax.numpy as jnp
from jax import lax
from jax.sharding import PartitionSpec as P

WIDTH = 3072
eps = 1e-06
residual_keep = 0.5


def causal_mix(gate_seq, conv_taps, conv_shift):
    count = conv_taps.shape[0]
    length = gate_seq.shape[1]
    padded = jnp.pad(gate_seq, ((0, 0), (count - 1, 0), (0, 0)))
    running = jnp.zeros_like(gate_seq) + conv_shift[None, None, :]
    for offset in range(count):
        running = (
            running + conv_taps[offset][None, None, :] * padded[:, offset : offset + length, :]
        )
    return running


def sublayer(current, norm_g, gate_w, gate_s, up_w, up_s, conv_taps, conv_shift, down_w, down_s):
    sequences, length, local_width = current.shape
    row_count = sequences * length
    values = current.astype(jnp.float32).reshape(row_count, local_width)
    squares = jnp.sum(values * values, axis=1)
    scaled = (values * norm_g[None, :]).astype(jnp.bfloat16)
    gate_part = jnp.dot(scaled, gate_w.astype(jnp.bfloat16), preferred_element_type=jnp.float32)
    up_part = jnp.dot(scaled, up_w.astype(jnp.bfloat16), preferred_element_type=jnp.float32)
    gate_sum, up_sum = (
        lax.psum_scatter(gate_part, "ra", scatter_dimension=1, tiled=True),
        lax.psum_scatter(up_part, "ra", scatter_dimension=1, tiled=True),
    )
    square_sum = lax.psum(squares, "ra")
    share_cols = gate_sum.shape[1]
    col_start = lax.axis_index("ra") * share_cols
    col_gate = lax.dynamic_slice_in_dim(gate_s, col_start, share_cols, 0)
    col_up = lax.dynamic_slice_in_dim(up_s, col_start, share_cols, 0)
    used_taps = lax.dynamic_slice_in_dim(conv_taps, col_start, share_cols, 1)
    used_shift = lax.dynamic_slice_in_dim(conv_shift, col_start, share_cols, 0)
    inverse_rms = lax.rsqrt(square_sum / WIDTH + eps)[:, None]
    gate_sum = gate_sum * inverse_rms * col_gate[None, :]
    up_sum = up_sum * inverse_rms * col_up[None, :]
    units = gate_sum.shape[1]
    conv_out = causal_mix(gate_sum.reshape(sequences, length, units), used_taps, used_shift)
    hidden_act = (jax.nn.silu(conv_out) * up_sum.reshape(sequences, length, units)).astype(
        jnp.bfloat16
    )
    hidden_act = hidden_act.reshape(row_count, units)
    hidden_act = lax.all_gather(hidden_act, "ra", axis=1, tiled=True)
    down_part = jnp.dot(hidden_act, down_w.astype(jnp.bfloat16), preferred_element_type=jnp.float32)
    down_sum = lax.psum(down_part, "cb")
    branch = down_sum * down_s[None, :]
    return (
        (residual_keep * values + branch)
        .astype(jnp.bfloat16)
        .reshape(sequences, length, local_width)
    )


def shards(
    tokens,
    norm_gain,
    gate_weight,
    gate_scale,
    up_weight,
    up_scale,
    conv_weight,
    conv_bias,
    down_weight,
    down_scale,
):
    current = tokens
    for layer_index in range(2):
        current = sublayer(
            current,
            norm_gain[layer_index],
            gate_weight[layer_index],
            gate_scale[layer_index],
            up_weight[layer_index],
            up_scale[layer_index],
            conv_weight[layer_index],
            conv_bias[layer_index],
            down_weight[layer_index],
            down_scale[layer_index],
        )
    return current


def solution(mesh):
    in_specs = (
        P(None, None, "ra"),
        P(None, "ra"),
        P(None, "ra", "cb"),
        P(None, "cb"),
        P(None, "ra", "cb"),
        P(None, "cb"),
        P(None, None, "cb"),
        P(None, "cb"),
        P(None, "cb", "ra"),
        P(None, "ra"),
    )
    out_specs = P(None, None, "ra")
    return jax.shard_map(shards, mesh=mesh, in_specs=in_specs, out_specs=out_specs, check_vma=False)
```

profile of v0, /device:TPU:0, one launch (start us, length us, event | category | flops | bytes accessed | tf_op | source)
XLA Modules:
  0.0 304.9 jit_solution(4028201805180705221)
XLA Ops:
  6.5 1.4 slice_reduce_fusion.1
  7.9 3.2 %convert.12 = bf16[2,768,1056]{1,2,0:T(8,128)(2,1)S(1)} convert(f32[2,768,1056]{1,2,0:T(8,128)} %param.12) | non-fusion elementwise | flops 1622016 | bytes 9732096 | tf_op jit(solution)/shard_map/convert.5
  11.1 1.2 convert_multiply_fusion.5
  13.1 1.6 fusion.5
  14.8 3.2 %convert.13 = bf16[2,768,1056]{1,2,0:T(8,128)(2,1)S(1)} convert(f32[2,768,1056]{1,2,0:T(8,128)} %param.14) | non-fusion elementwise | flops 1622016 | bytes 9732096 | tf_op jit(solution)/shard_map/convert.4
  17.9 1.7 copy-done.1
  19.6 1.6 fusion.4
  21.4 3.4 %convert.14 = bf16[2,1056,768]{2,1,0:T(8,128)(2,1)S(1)} convert(f32[2,1056,768]{2,1,0:T(8,128)} %param.18) | non-fusion elementwise | flops 1622016 | bytes 9732096 | tf_op jit(solution)/shard_map/convert.3
  26.9 13.9 %psum.28 = f32[256]{0:T(256)S(1)} all-reduce(f32[256]{0:T(256)S(1)} %bitcast.56), channel_id=1, replica_groups=mesh['ra'=4,'cb'=8] {'ra'}, use_global_device_ids=true, to_apply=%region_2.0 | all-reduce | flops 256 | bytes 2048 | tf_op jit(solution)/shard_map/psum | solution.py:35
  41.4 4.3 %reduce-scatter.5.cloned.1.call-done = f32[256,264]{0,1:T(8,128)} async-done(((f32[256,1056]{0,1:T(8,128)}), f32[256,264]{0,1:T(8,128)}) %reduce-scatter.5.cloned.1.call-update) | async-done | bytes 270352 | tf_op jit(solution)/shard_map/reduce_scatter | solution.py:32
  45.7 28.7 %reduce-scatter.7.cloned.1.call-done = f32[256,264]{0,1:T(8,128)} async-done(((f32[256,1056]{0,1:T(8,128)}), f32[256,264]{0,1:T(8,128)}) %reduce-scatter.7.cloned.1.call-update) | async-done | bytes 270352 | tf_op jit(solution)/shard_map/reduce_scatter | solution.py:33
  74.3 1.9 multiply_multiply_fusion.3
  76.2 1.8 reshape.75
  78.0 0.8 reshape.76
  78.8 3.7 %fusion.28 = bf16[2,128,264]{1,0,2:T(2,128)(2,1)S(1)} fusion(f32[2,128,264]{1,0,2:T(2,128)} %reshape.76, f32[2,128,264]{1,0,2:T(2,128)} %reshape.75, f32[264]{0:T(512)} %get-tuple-element.10, f32[264]{0:T(512)S(1)} %get-tuple-element.9, f32[264]{0:T(512)S(1)} %get-tuple-element.8, f32[264]{0:T(512)S(1)} %get-tuple-element.32), kind=kLoop, calls=%fused_computation.49 | loop fusion | flops 811008 | bytes 680064 | tf_op jit(solution)/shard_map/convert_element_type | solution.py:47
  82.6 16.0 %all_gather.6 = bf16[256,1056]{0,1:T(8,128)(2,1)S(1)} all-gather(bf16[256,264]{0,1:T(8,128)(2,1)S(1)} %bitcast.54), channel_id=1, replica_groups=mesh['ra'=4,'cb'=8] {'ra'}, dimensions={1}, use_global_device_ids=true | all-gather | bytes 675840 | tf_op jit(solution)/shard_map/all_gather | solution.py:51
  98.6 1.6 fusion.3
  100.3 54.1 %all-reduce.5.cloned.1.call-done = f32[256,768]{1,0:T(8,128)} async-done(((f32[256,768]{1,0:T(8,128)}), f32[256,768]{1,0:T(8,128)}) %all-reduce.5.cloned.1.call-update) | async-done | bytes 786448 | tf_op jit(solution)/shard_map/psum | solution.py:53
  154.4 1.6 fusion.11
  156.7 3.1 %fusion.1 = f32[256,1056]{0,1:T(8,128)} fusion(bf16[2,768,1056]{1,2,0:T(8,128)(2,1)} %copy-done.1, bf16[256,768]{1,0:T(8,128)(2,1)S(1)} %get-tuple-element.16, f32[768]{0:T(1024)S(1)} %copy-done.9), kind=kOutput, calls=%fused_computation.3 | convolution fusion | flops 415825920 | bytes 3099648 | tf_op jit(solution)/shard_map/dot_general | solution.py:30
  159.9 3.2 %fusion.2 = f32[256,1056]{0,1:T(8,128)} fusion(bf16[2,768,1056]{1,2,0:T(8,128)(2,1)} %copy-done, bf16[256,768]{1,0:T(8,128)(2,1)} %copy-done.2, f32[768]{0:T(1024)S(1)} %copy-done.9), kind=kOutput, calls=%fused_computation.5 | convolution fusion | flops 415825920 | bytes 3099648 | tf_op jit(solution)/shard_map/dot_general | solution.py:29
  163.1 1.4 fusion.35
  164.6 12.2 %psum.30 = f32[256]{0:T(256)S(1)} all-reduce(f32[256]{0:T(256)S(1)} %get-tuple-element.15), channel_id=1, replica_groups=mesh['ra'=4,'cb'=8] {'ra'}, use_global_device_ids=true, to_apply=%region_7.8 | all-reduce | flops 256 | bytes 2048 | tf_op jit(solution)/shard_map/psum | solution.py:35
  176.8 10.4 %reduce-scatter.11.cloned.1.call-done = f32[256,264]{0,1:T(8,128)} async-done(((f32[256,1056]{0,1:T(8,128)}), f32[256,264]{0,1:T(8,128)}) %reduce-scatter.11.cloned.1.call-update) | async-done | bytes 270352 | tf_op jit(solution)/shard_map/reduce_scatter | solution.py:33
  187.2 28.5 %reduce-scatter.9.cloned.1.call-done = f32[256,264]{0,1:T(8,128)} async-done(((f32[256,1056]{0,1:T(8,128)}), f32[256,264]{0,1:T(8,128)}) %reduce-scatter.9.cloned.1.call-update) | async-done | bytes 270352 | tf_op jit(solution)/shard_map/reduce_scatter | solution.py:32
  215.8 1.9 multiply_multiply_fusion.1
  217.6 1.8 reshape.78
  220.3 3.7 %fusion.27 = bf16[2,128,264]{1,0,2:T(2,128)(2,1)S(1)} fusion(f32[2,128,264]{1,0,2:T(2,128)} %reshape.79, f32[2,128,264]{1,0,2:T(2,128)} %reshape.78, f32[264]{0:T(512)S(1)} %get-tuple-element.7, f32[264]{0:T(512)S(1)} %get-tuple-element.6, f32[264]{0:T(512)S(1)} %get-tuple-element.5, f32[264]{0:T(512)S(1)} %get-tuple-element.33), kind=kLoop, calls=%fused_computation.48 | loop fusion | flops 811008 | bytes 680064 | tf_op jit(solution)/shard_map/convert_element_type | solution.py:47
  224.0 16.0 %all_gather.7 = bf16[256,1056]{0,1:T(8,128)(2,1)S(1)} all-gather(bf16[256,264]{0,1:T(8,128)(2,1)S(1)} %bitcast.55), channel_id=1, replica_groups=mesh['ra'=4,'cb'=8] {'ra'}, dimensions={1}, use_global_device_ids=true | all-gather | bytes 675840 | tf_op jit(solution)/shard_map/all_gather | solution.py:51
  240.0 1.6 fusion
  241.6 54.3 %all-reduce.7.cloned.1.call-done = f32[256,768]{1,0:T(8,128)} async-done(((f32[256,768]{1,0:T(8,128)}), f32[256,768]{1,0:T(8,128)}) %all-reduce.7.cloned.1.call-update) | async-done | bytes 786448 | tf_op jit(solution)/shard_map/psum | solution.py:53
  295.9 2.1 fusion.9
  (45 shorter events, 5.4 us)
Async XLA Ops:
  6.5 39.1 %reduce-scatter.5.cloned.1.call-start = ((), (), s32[]{:S(2)}) async-start(), calls=%async_computation.4 | async-start | bytes 1351680 | tf_op jit(solution)/shard_map/reduce_scatter | solution.py:32
  7.9 3.2 %copy-start.3 = (bf16[2,128,768]{2,1,0:T(8,128)(2,1)S(1)}, bf16[2,128,768]{2,1,0:T(8,128)(2,1)}, u32[]{:S(2)}) copy-start(bf16[2,128,768]{2,1,0:T(8,128)(2,1)} %param.10) | copy-start | bytes 1179652
  11.1 1.9 copy-start
  14.7 59.6 %reduce-scatter.7.cloned.1.call-start = ((), (), s32[]{:S(2)}) async-start(), calls=%async_computation.5 | async-start | bytes 1351680 | tf_op jit(solution)/shard_map/reduce_scatter | solution.py:33
  17.9 1.7 copy-start.1
  21.3 133.1 %all-reduce.5.cloned.1.call-start = ((), (), s32[]{:S(2)}) async-start(), calls=%async_computation.6 | async-start | bytes 1572864 | tf_op jit(solution)/shard_map/psum | solution.py:53
  21.4 3.4 %copy-start.5 = (f32[2,1056]{1,0:T(2,128)S(1)}, f32[2,1056]{1,0:T(2,128)}, u32[]{:S(2)}) copy-start(f32[2,1056]{1,0:T(2,128)} %param.13) | copy-start | bytes 25348
  21.4 4.0 %copy-start.6 = (f32[2,1056]{1,0:T(2,128)S(1)}, f32[2,1056]{1,0:T(2,128)}, u32[]{:S(2)}) copy-start(f32[2,1056]{1,0:T(2,128)} %param.15) | copy-start | bytes 25348
  21.4 4.7 %copy-start.7 = (f32[2,1056]{1,0:T(2,128)S(1)}, f32[2,1056]{1,0:T(2,128)}, u32[]{:S(2)}) copy-start(f32[2,1056]{1,0:T(2,128)} %param.17) | copy-start | bytes 25348
  21.4 4.8 %copy-start.4 = (f32[2,3,1056]{2,0,1:T(2,128)S(1)}, f32[2,3,1056]{2,0,1:T(2,128)}, u32[]{:S(2)}) copy-start(f32[2,3,1056]{2,0,1:T(2,128)} %param.16) | copy-start | bytes 76036
  98.6 1.7 copy-start.8
  100.2 56.5 %copy-start.9 = (f32[768]{0:T(1024)S(1)}, f32[768]{0:T(1024)}, u32[]{:S(2)}) copy-start(f32[768]{0:T(1024)} %get-tuple-element.13) | copy-start | bytes 9220
  100.2 87.0 %reduce-scatter.11.cloned.1.call-start = ((), (), s32[]{:S(2)}) async-start(), calls=%async_computation.8 | async-start | bytes 1351680 | tf_op jit(solution)/shard_map/reduce_scatter | solution.py:33
  156.0 0.7 copy-start.2
  159.8 56.0 %reduce-scatter.9.cloned.1.call-start = ((), (), s32[]{:S(2)}) async-start(), calls=%async_computation.7 | async-start | bytes 1351680 | tf_op jit(solution)/shard_map/reduce_scatter | solution.py:32
  163.1 132.8 %all-reduce.7.cloned.1.call-start = ((), (), s32[]{:S(2)}) async-start(), calls=%async_computation.9 | async-start | bytes 1572864 | tf_op jit(solution)/shard_map/psum | solution.py:53
Sparse Core Ops, SparseCore 0:
  14.8 30.7 reduce-scatter.4
  48.0 26.3 reduce-scatter.6
  100.4 53.9 all-reduce.4
  159.9 27.2 reduce-scatter.10
  189.4 26.3 reduce-scatter.8
  241.8 54.0 all-reduce.6
where the time goes:
time: 306 us; the launch traced here: 305 us
  waiting for transfers between devices  180 us (59%)
  blocking collectives  58.2 us (19%)
  other arithmetic  26.3 us (9%)
  between operations  13.7 us (4%)
  local copies, waits for them, and re-layouts  13.4 us (4%)
  matrix products  12.7 us (4%)
    psum x2, waiting for transfers between devices, sublayer(): down_sum = lax.psum(down_part, 'cb')  108 us
    reduce_scatter x2, waiting for transfers between devices, sublayer(): lax.psum_scatter(up_part, 'ra', scatter_dimension=1, tiled=True)  39.1 us
    reduce_scatter x2, waiting for transfers between devices, sublayer(): lax.psum_scatter(gate_part, 'ra', scatter_dimension=1, tiled=True)  32.8 us
    all_gather x2, blocking collectives, sublayer(): hidden_act = lax.all_gather(hidden_act, 'ra', axis=1, tiled=True)  32 us
    psum x2, blocking collectives, sublayer(): square_sum = lax.psum(squares, 'ra')  26.1 us
    another operation x3, other arithmetic  9.73 us
    convert_element_type x2, other arithmetic, sublayer(): (jax.nn.silu(conv_out) * up_sum.reshape(sequences, length, units)).astype...  7.42 us
  transfers between devices with their start and end apart: 6, of which 6 were waited for; matrix products, arithmetic and copies ran while one was open for 5% of the time, Pallas kernels for 0%

commit v1 on v0

--- a/solution.py
+++ b/solution.py
@@ -50,7 +50,7 @@
     hidden_act = hidden_act.reshape(row_count, units)
     hidden_act = lax.all_gather(hidden_act, "ra", axis=1, tiled=True)
     down_part = jnp.dot(hidden_act, down_w.astype(jnp.bfloat16), preferred_element_type=jnp.float32)
-    down_sum = lax.psum(down_part, "cb")
+    down_sum = jnp.sum(lax.all_gather(down_part, "cb"), axis=0)
     branch = down_sum * down_s[None, :]
     return (
         (residual_keep * values + branch)

time: 306 us -> 292 us (0.954)
  waiting for transfers between devices: 180 us -> 161 us
  other arithmetic: 26.3 us -> 31.6 us
    psum x2 -> x0, waiting for transfers between devices: 108 us -> none  [sublayer(): down_sum = lax.psum(down_part, 'cb')]
    all_gather x0 -> x2, waiting for transfers between devices: none -> 87.9 us  [sublayer(): down_sum = jnp.sum(lax.all_gather(down_part, 'cb'), axis=0)]
    reduce_scatter x2, waiting for transfers between devices: 39.1 us -> 57.1 us  [sublayer(): lax.psum_scatter(up_part, 'ra', scatter_dimension=1, tiled=True)]
    reduce_scatter x2, waiting for transfers between devices: 32.8 us -> 15.5 us  [sublayer(): lax.psum_scatter(gate_part, 'ra', scatter_dimension=1, tiled=True)]
    reduce_sum x0 -> x2, other arithmetic: none -> 7.46 us  [sublayer(): down_sum = jnp.sum(lax.all_gather(down_part, 'cb'), axis=0)]
where the time goes in v1:
time: 292 us; the launch traced here: 291 us
  waiting for transfers between devices  161 us (55%)
  blocking collectives  58.1 us (20%)
  other arithmetic  31.6 us (11%)
  local copies, waits for them, and re-layouts  13.8 us (5%)
  between operations  13.7 us (5%)
  matrix products  12.8 us (4%)
    all_gather x2, waiting for transfers between devices, sublayer(): down_sum = jnp.sum(lax.all_gather(down_part, 'cb'), axis=0)  87.9 us
    reduce_scatter x2, waiting for transfers between devices, sublayer(): lax.psum_scatter(up_part, 'ra', scatter_dimension=1, tiled=True)  57.1 us
    all_gather x2, blocking collectives, sublayer(): hidden_act = lax.all_gather(hidden_act, 'ra', axis=1, tiled=True)  32 us
    psum x2, blocking collectives, sublayer(): square_sum = lax.psum(squares, 'ra')  26.1 us
    reduce_scatter x2, waiting for transfers between devices, sublayer(): lax.psum_scatter(gate_part, 'ra', scatter_dimension=1, tiled=True)  15.5 us
    another operation x3, other arithmetic  9.78 us
    reduce_sum x2, other arithmetic, sublayer(): down_sum = jnp.sum(lax.all_gather(down_part, 'cb'), axis=0)  7.46 us
    convert_element_type x2, other arithmetic, sublayer(): (jax.nn.silu(conv_out) * up_sum.reshape(sequences, length, units)).astype...  7.43 us
  transfers between devices with their start and end apart: 6, of which 6 were waited for; matrix products, arithmetic and copies ran while one was open for 5% of the time, Pallas kernels for 0%

profile of v1, /device:TPU:0, one launch (start us, length us, event | category | flops | bytes accessed | tf_op | source)
XLA Modules:
  0.0 290.8 jit_solution(17911828176781684965)
XLA Ops:
  7.3 3.2 %convert.12 = bf16[2,768,1056]{1,2,0:T(8,128)(2,1)S(1)} convert(f32[2,768,1056]{1,2,0:T(8,128)} %param.12) | non-fusion elementwise | flops 1622016 | bytes 9732096 | tf_op jit(solution)/shard_map/convert.5
  10.8 0.9 copy-done.2
  11.7 1.6 fusion.5
  13.4 3.2 %convert.13 = bf16[2,768,1056]{1,2,0:T(8,128)(2,1)S(1)} convert(f32[2,768,1056]{1,2,0:T(8,128)} %param.14) | non-fusion elementwise | flops 1622016 | bytes 9732096 | tf_op jit(solution)/shard_map/convert.4
  16.6 1.7 copy-done.1
  18.3 1.6 fusion.4
  20.1 3.4 %convert.14 = bf16[2,1056,768]{2,1,0:T(8,128)(2,1)S(1)} convert(f32[2,1056,768]{2,1,0:T(8,128)} %param.18) | non-fusion elementwise | flops 1622016 | bytes 9732096 | tf_op jit(solution)/shard_map/convert.3
  25.6 13.9 %psum.14 = f32[256]{0:T(256)S(1)} all-reduce(f32[256]{0:T(256)S(1)} %bitcast.64), channel_id=1, replica_groups=mesh['ra'=4,'cb'=8] {'ra'}, use_global_device_ids=true, to_apply=%region_2.0 | all-reduce | flops 256 | bytes 2048 | tf_op jit(solution)/shard_map/psum | solution.py:35
  40.0 4.3 %reduce-scatter.5.cloned.1.call-done = f32[256,264]{0,1:T(8,128)} async-done(((f32[256,1056]{0,1:T(8,128)}), f32[256,264]{0,1:T(8,128)}) %reduce-scatter.5.cloned.1.call-update) | async-done | bytes 270352 | tf_op jit(solution)/shard_map/reduce_scatter | solution.py:32
  44.3 28.7 %reduce-scatter.7.cloned.1.call-done = f32[256,264]{0,1:T(8,128)} async-done(((f32[256,1056]{0,1:T(8,128)}), f32[256,264]{0,1:T(8,128)}) %reduce-scatter.7.cloned.1.call-update) | async-done | bytes 270352 | tf_op jit(solution)/shard_map/reduce_scatter | solution.py:33
  73.0 1.9 multiply_multiply_fusion.3
  74.8 1.8 reshape.96
  77.5 3.7 %fusion.27 = bf16[2,128,264]{1,0,2:T(2,128)(2,1)S(1)} fusion(f32[2,128,264]{1,0,2:T(2,128)} %reshape.97, f32[2,128,264]{1,0,2:T(2,128)} %reshape.96, f32[264]{0:T(512)} %get-tuple-element.10, f32[264]{0:T(512)} %get-tuple-element.9, f32[264]{0:T(512)S(1)} %get-tuple-element.8, f32[264]{0:T(512)S(1)} %get-tuple-element.31), kind=kLoop, calls=%fused_computation.49 | loop fusion | flops 811008 | bytes 680064 | tf_op jit(solution)/shard_map/convert_element_type | solution.py:47
  81.3 16.0 %all_gather.18 = bf16[256,1056]{0,1:T(8,128)(2,1)S(1)} all-gather(bf16[256,264]{0,1:T(8,128)(2,1)S(1)} %bitcast.62), channel_id=1, replica_groups=mesh['ra'=4,'cb'=8] {'ra'}, dimensions={1}, use_global_device_ids=true | all-gather | bytes 675840 | tf_op jit(solution)/shard_map/all_gather | solution.py:51
  97.3 1.7 fusion.3
  99.1 43.9 %all-gather.5.cloned.1.call-done = f32[2048,768]{1,0:T(8,128)} async-done(((f32[256,768]{1,0:T(8,128)}), f32[2048,768]{1,0:T(8,128)}) %all-gather.5.cloned.1.call-update) | async-done | bytes 6291472 | tf_op jit(solution)/shard_map/all_gather | solution.py:53
  142.9 4.2 %reduce_sum.46 = f32[256,768]{1,0:T(8,128)} reduce(f32[8,256,768]{2,1,0:T(8,128)} %bitcast.52, f32[]{:T(128)} %constant.30.clone.1), dimensions={0}, to_apply=%region_4.5 | reduce | flops 1376256 | bytes 7077892 | tf_op jit(solution)/shard_map/reduce_sum | solution.py:53
  147.1 1.5 fusion.13
  150.2 3.0 %fusion.2 = f32[256,1056]{0,1:T(8,128)} fusion(bf16[256,768]{1,0:T(8,128)(2,1)S(1)} %bitcast.56, bf16[2,768,1056]{1,2,0:T(8,128)(2,1)} %copy-done), kind=kOutput, calls=%fused_computation.5 | convolution fusion | flops 415236096 | bytes 3096576 | tf_op jit(solution)/shard_map/dot_general | solution.py:29
  153.3 3.2 %fusion.1 = f32[256,1056]{0,1:T(8,128)} fusion(bf16[256,768]{1,0:T(8,128)(2,1)} %bitcast.57, bf16[2,768,1056]{1,2,0:T(8,128)(2,1)} %copy-done.1), kind=kOutput, calls=%fused_computation.3 | convolution fusion | flops 415236096 | bytes 3096576 | tf_op jit(solution)/shard_map/dot_general | solution.py:30
  156.6 1.4 fusion.34
  158.0 12.2 %psum.15 = f32[256]{0:T(256)S(1)} all-reduce(f32[256]{0:T(256)S(1)} %bitcast.65), channel_id=1, replica_groups=mesh['ra'=4,'cb'=8] {'ra'}, use_global_device_ids=true, to_apply=%region_7.8 | all-reduce | flops 256 | bytes 2048 | tf_op jit(solution)/shard_map/psum | solution.py:35
  170.2 11.2 %reduce-scatter.9.cloned.1.call-done = f32[256,264]{0,1:T(8,128)} async-done(((f32[256,1056]{0,1:T(8,128)}), f32[256,264]{0,1:T(8,128)}) %reduce-scatter.9.cloned.1.call-update) | async-done | bytes 270352 | tf_op jit(solution)/shard_map/reduce_scatter | solution.py:32
  181.4 28.5 %reduce-scatter.11.cloned.1.call-done = f32[256,264]{0,1:T(8,128)} async-done(((f32[256,1056]{0,1:T(8,128)}), f32[256,264]{0,1:T(8,128)}) %reduce-scatter.11.cloned.1.call-update) | async-done | bytes 270352 | tf_op jit(solution)/shard_map/reduce_scatter | solution.py:33
  209.9 1.9 multiply_multiply_fusion.1
  211.8 1.8 reshape.99
  214.4 3.7 %fusion.26 = bf16[2,128,264]{1,0,2:T(2,128)(2,1)S(1)} fusion(f32[2,128,264]{1,0,2:T(2,128)} %reshape.100, f32[2,128,264]{1,0,2:T(2,128)} %reshape.99, f32[264]{0:T(512)S(1)} %get-tuple-element.7, f32[264]{0:T(512)S(1)} %get-tuple-element.6, f32[264]{0:T(512)S(1)} %get-tuple-element.5, f32[264]{0:T(512)S(1)} %get-tuple-element.32), kind=kLoop, calls=%fused_computation.48 | loop fusion | flops 811008 | bytes 680064 | tf_op jit(solution)/shard_map/convert_element_type | solution.py:47
  218.1 16.0 %all_gather.21 = bf16[256,1056]{0,1:T(8,128)(2,1)S(1)} all-gather(bf16[256,264]{0,1:T(8,128)(2,1)S(1)} %bitcast.63), channel_id=1, replica_groups=mesh['ra'=4,'cb'=8] {'ra'}, dimensions={1}, use_global_device_ids=true | all-gather | bytes 675840 | tf_op jit(solution)/shard_map/all_gather | solution.py:51
  234.2 1.6 fusion
  235.8 44.0 %all-gather.7.cloned.1.call-done = f32[2048,768]{1,0:T(8,128)} async-done(((f32[256,768]{1,0:T(8,128)}), f32[2048,768]{1,0:T(8,128)}) %all-gather.7.cloned.1.call-update) | async-done | bytes 6291472 | tf_op jit(solution)/shard_map/all_gather | solution.py:53
  279.8 3.3 %reduce_sum.50 = f32[256,768]{1,0:T(8,128)S(1)} reduce(f32[8,256,768]{2,1,0:T(8,128)} %bitcast.53, f32[]{:T(128)} %constant.30.clone.1), dimensions={0}, to_apply=%region_9.10 | reduce | flops 1376256 | bytes 7077892 | tf_op jit(solution)/shard_map/reduce_sum | solution.py:53
  283.0 0.9 fusion.11
  (54 shorter events, 7.4 us)
Async XLA Ops:
  6.5 37.8 %reduce-scatter.5.cloned.1.call-start = ((), (), s32[]{:S(2)}) async-start(), calls=%async_computation.4 | async-start | bytes 1351680 | tf_op jit(solution)/shard_map/reduce_scatter | solution.py:32
  7.3 3.2 %copy-start.7 = (bf16[2,128,768]{2,1,0:T(8,128)(2,1)S(1)}, bf16[2,128,768]{2,1,0:T(8,128)(2,1)}, u32[]{:S(2)}) copy-start(bf16[2,128,768]{2,1,0:T(8,128)(2,1)} %param.10) | copy-start | bytes 1179652
  10.6 9.5 %copy-start = (bf16[2,768,1056]{1,2,0:T(8,128)(2,1)}, bf16[2,768,1056]{1,2,0:T(8,128)(2,1)S(1)}, u32[]{:S(2)}) copy-start(bf16[2,768,1056]{1,2,0:T(8,128)(2,1)S(1)} %convert.12) | copy-start | bytes 9732100
  10.8 1.0 copy-start.2
  13.4 59.6 %reduce-scatter.7.cloned.1.call-start = ((), (), s32[]{:S(2)}) async-start(), calls=%async_computation.5 | async-start | bytes 1351680 | tf_op jit(solution)/shard_map/reduce_scatter | solution.py:33
  13.4 4.9 %copy-start.3 = (bf16[2,128,768]{2,1,0:T(8,128)(2,1)S(1)}, bf16[2,128,768]{2,1,0:T(8,128)(2,1)}, u32[]{:S(2)}) copy-start(bf16[2,128,768]{2,1,0:T(8,128)(2,1)} %copy-done.2) | copy-start | bytes 1179652
  16.6 1.7 copy-start.1
  20.0 123.0 %all-gather.5.cloned.1.call-start = ((), (), s32[]{:S(2)}) async-start(), calls=%async_computation.8 | async-start | bytes 7077888 | tf_op jit(solution)/shard_map/all_gather | solution.py:53
  20.0 3.4 %copy-start.9 = (f32[2,1056]{1,0:T(2,128)S(1)}, f32[2,1056]{1,0:T(2,128)}, u32[]{:S(2)}) copy-start(f32[2,1056]{1,0:T(2,128)} %param.13) | copy-start | bytes 25348
  20.1 4.0 %copy-start.10 = (f32[2,1056]{1,0:T(2,128)S(1)}, f32[2,1056]{1,0:T(2,128)}, u32[]{:S(2)}) copy-start(f32[2,1056]{1,0:T(2,128)} %param.15) | copy-start | bytes 25348
  20.1 4.7 %copy-start.11 = (f32[2,1056]{1,0:T(2,128)S(1)}, f32[2,1056]{1,0:T(2,128)}, u32[]{:S(2)}) copy-start(f32[2,1056]{1,0:T(2,128)} %param.17) | copy-start | bytes 25348
  20.1 4.8 %copy-start.8 = (f32[2,3,1056]{2,0,1:T(2,128)S(1)}, f32[2,3,1056]{2,0,1:T(2,128)}, u32[]{:S(2)}) copy-start(f32[2,3,1056]{2,0,1:T(2,128)} %param.16) | copy-start | bytes 76036
  74.8 24.2 %copy-start.12 = (f32[2,768]{1,0:T(2,128)S(1)}, f32[2,768]{1,0:T(2,128)}, u32[]{:S(2)}) copy-start(f32[2,768]{1,0:T(2,128)} %param.19) | copy-start | bytes 18436
  99.0 82.5 %reduce-scatter.9.cloned.1.call-start = ((), (), s32[]{:S(2)}) async-start(), calls=%async_computation.6 | async-start | bytes 1351680 | tf_op jit(solution)/shard_map/reduce_scatter | solution.py:32
  148.6 0.7 copy-start.5
  149.4 0.7 copy-start.4
  153.2 56.7 %reduce-scatter.11.cloned.1.call-start = ((), (), s32[]{:S(2)}) async-start(), calls=%async_computation.7 | async-start | bytes 1351680 | tf_op jit(solution)/shard_map/reduce_scatter | solution.py:33
  156.5 123.2 %all-gather.7.cloned.1.call-start = ((), (), s32[]{:S(2)}) async-start(), calls=%async_computation.9 | async-start | bytes 7077888 | tf_op jit(solution)/shard_map/all_gather | solution.py:53
  279.7 3.3 %copy-start.6 = (bf16[2,128,768]{2,1,0:T(8,128)(2,1)S(1)}, bf16[2,128,768]{2,1,0:T(8,128)(2,1)}, u32[]{:S(2)}) copy-start(bf16[2,128,768]{2,1,0:T(8,128)(2,1)} %copy-done.5) | copy-start | bytes 1179652
Sparse Core Ops, SparseCore 0:
  13.5 30.7 reduce-scatter.4
  46.6 26.3 reduce-scatter.6
  99.1 43.8 all-gather.4
  153.3 28.0 reduce-scatter.8
  183.6 26.2 reduce-scatter.10
  235.9 43.8 all-gather.6
